TPU v7x, 32 devices: a whole 2x2x4 slice. The times are simulated.
32 devices in a mesh: fs: 16 (over z, y, x), tp: 2 (over core).
Axes of the slice: x: 2, y: 2, z: 4, core: 2. Of those that a mesh axis runs over, the one named last changes fastest.
Arguments:
- normed_input: bfloat16 [8192, 2048], P('fs', 'tp'), may hold values from -6 to 6
- cotangent: bfloat16 [8192, 2048], P('fs', 'tp'), may hold values from -6 to 6
- up_weight: bfloat16 [2048, 8192], P('fs', 'tp'), may hold values from -0.125 to 0.125
- down_weight: bfloat16 [8192, 2048], P('tp', 'fs'), may hold values from -0.0625 to 0.0625
Outputs:
- input_grad: bfloat16 [8192, 2048], P('fs', 'tp')
- up_grad: float32 [2048, 8192], P('fs', 'tp')
- down_grad: float32 [8192, 2048], P('tp', 'fs')
All inputs are finite; a program needn't handle non-finite values.
Results may differ from a plain program's by a relative error of at most 0.018.
Values may be sent and summed in bfloat16 or wider, within the bound.
A program may use at most 192 MiB of HBM per device.

v0:
```python
import jax
import jax.numpy as jnp
from jax import lax
from jax.sharding import PartitionSpec as P


def right_product(left, right):
    return lax.dot_general(
        left, right, (((1,), (1,)), ((), ())), preferred_element_type=jnp.float32
    )


def left_product(left, right):
    return lax.dot_general(
        left, right, (((0,), (0,)), ((), ())), preferred_element_type=jnp.float32
    )


def per_device(normed_input, cotangent, up_weight, down_weight):
    whole_input, whole_cot = (
        lax.all_gather(normed_input, "tp", axis=1, tiled=True),
        lax.all_gather(cotangent, "tp", axis=1, tiled=True),
    )
    rows = whole_input.shape[0]
    tokens = rows * lax.axis_size("fs")
    scale = lax.rsqrt(jnp.asarray(tokens, jnp.float32))
    block = whole_cot
    act_grad = right_product(block, lax.all_gather(down_weight, "fs", axis=1, tiled=True))
    whole_up = lax.all_gather(up_weight, "fs", axis=0, tiled=True)
    pre = jnp.dot(whole_input, whole_up, preferred_element_type=jnp.float32)
    rectified = jax.nn.relu(pre)
    act = (rectified * rectified).astype(jnp.bfloat16)
    pre_grad = (2.0 * rectified * act_grad).astype(jnp.bfloat16)
    partial_value = right_product(pre_grad, whole_up)
    input_grad = lax.psum_scatter(
        partial_value.astype(jnp.bfloat16), "tp", scatter_dimension=1, tiled=True
    )
    block = whole_input
    up_grad = lax.psum_scatter(
        (left_product(block, pre_grad) * scale).astype(jnp.bfloat16),
        "fs",
        scatter_dimension=0,
        tiled=True,
    ).astype(jnp.float32)
    down_term = left_product(act, whole_cot) * scale
    down_grad = lax.psum_scatter(
        down_term.astype(jnp.bfloat16), "fs", scatter_dimension=1, tiled=True
    ).astype(jnp.float32)
    return (input_grad, up_grad, down_grad)


def solution(mesh):
    in_specs = (P("fs", "tp"), P("fs", "tp"), P("fs", "tp"), P("tp", "fs"))
    out_specs = (P("fs", "tp"), P("fs", "tp"), P("tp", "fs"))
    return jax.shard_map(
        per_device, mesh=mesh, in_specs=in_specs, out_specs=out_specs, check_vma=False
    )
```

profile of v0, /device:TPU:0, one launch (start us, length us, event | category | flops | bytes accessed | tf_op | source)
XLA Modules:
  0.0 1207.0 jit_solution(5225547359864163482)
XLA Ops:
  7.2 0.7 all-gather.5.cloned.1.call-update
  7.9 0.7 all-gather.7.cloned.1.call-update
  8.7 0.7 all-gather.9.cloned.1.call-update
  9.4 0.5 all-gather.11.cloned.1.call-update
  10.0 0.0 reduce-scatter.12.cloned.1.call-start
  10.0 12.8 %all-gather.5.cloned.1.call-done = bf16[512,2048]{1,0:T(8,128)(2,1)} async-done(((bf16[512,1024]{1,0:T(8,128)(2,1)}), bf16[512,2048]{1,0:T(8,128)(2,1)}) %all-gather.5.cloned.1.call-update) | async-done | bytes 2097168 | tf_op jit(solution)/shard_map/all_gather | solution.py:21
  22.8 195.0 %all-gather.7.cloned.1.call-done = bf16[2048,4096]{1,0:T(8,128)(2,1)} async-done(((bf16[128,4096]{1,0:T(8,128)(2,1)}), bf16[2048,4096]{1,0:T(8,128)(2,1)}) %all-gather.7.cloned.1.call-update) | async-done | bytes 16777232 | tf_op jit(solution)/shard_map/all_gather | solution.py:29
  217.8 14.9 %fusion.3 = f32[512,4096]{1,0:T(8,128)} fusion(bf16[512,2048]{1,0:T(8,128)(2,1)} %all-gather.5.cloned.1.call-done, bf16[2048,4096]{1,0:T(8,128)(2,1)} %all-gather.7.cloned.1.call-done), kind=kOutput, calls=%fused_computation.8 | convolution fusion | flops 8589934592 | bytes 27262976 | tf_op jit(solution)/shard_map/dot_general | solution.py:30
  232.7 16.2 %multiply_convert_fusion = bf16[4096,2048]{1,0:T(8,128)(2,1)} fusion(bf16[512,2048]{1,0:T(8,128)(2,1)} %all-gather.9.cloned.1.call-done, f32[512,4096]{1,0:T(8,128)} %fusion.3), kind=kOutput, calls=%fused_computation | convolution fusion | flops 8613003264 | bytes 27262976 | tf_op jit(solution)/shard_map/dot_general | solution.py:14
  248.9 21.5 %copy.11 = bf16[4096,2048]{0,1:T(8,128)(2,1)} copy(bf16[4096,2048]{1,0:T(8,128)(2,1)} %multiply_convert_fusion) | data formatting | bytes 33554432
  270.5 0.2 reduce-scatter.10.cloned.1.call-start
  270.7 210.3 %all-gather.11.cloned.1.call-done = bf16[4096,2048]{1,0:T(8,128)(2,1)} async-done(((bf16[4096,128]{1,0:T(8,128)(2,1)}), bf16[4096,2048]{1,0:T(8,128)(2,1)}) %all-gather.11.cloned.1.call-update) | async-done | bytes 16777232 | tf_op jit(solution)/shard_map/all_gather | solution.py:28
  481.0 15.6 %multiply_convert_fusion.3 = bf16[512,4096]{1,0:T(8,128)(2,1)} fusion(f32[512,4096]{1,0:T(8,128)} %fusion.3, bf16[512,2048]{1,0:T(8,128)(2,1)} %all-gather.9.cloned.1.call-done, bf16[4096,2048]{1,0:T(8,128)(2,1)} %all-gather.11.cloned.1.call-done), kind=kOutput, calls=%fused_computation.4 | convolution fusion | flops 8598323200 | bytes 31457280 | tf_op jit(solution)/shard_map/dot_general | solution.py:8
  496.6 14.8 %fusion = bf16[2048,4096]{0,1:T(8,128)(2,1)} fusion(bf16[512,4096]{1,0:T(8,128)(2,1)} %multiply_convert_fusion.3, bf16[512,2048]{1,0:T(8,128)(2,1)S(1)} %copy-done), kind=kOutput, calls=%fused_computation.2 | convolution fusion | flops 8606711808 | bytes 23068672 | tf_op jit(solution)/shard_map/dot_general | solution.py:14
  511.4 21.4 %copy.9 = bf16[2048,4096]{1,0:T(8,128)(2,1)} copy(bf16[2048,4096]{0,1:T(8,128)(2,1)} %fusion) | data formatting | bytes 33554432
  532.8 0.3 reduce-scatter.8.cloned.1.call-start
  533.1 14.8 %convolution_convert_fusion = bf16[512,2048]{1,0:T(8,128)(2,1)} fusion(bf16[512,4096]{1,0:T(8,128)(2,1)} %multiply_convert_fusion.3, bf16[2048,4096]{1,0:T(8,128)(2,1)} %all-gather.7.cloned.1.call-done), kind=kOutput, calls=%fused_computation.6 | convolution fusion | flops 8590983168 | bytes 23068672 | tf_op jit(solution)/shard_map/dot_general | solution.py:8
  547.9 279.9 %reduce-scatter.12.cloned.1.call-done = bf16[128,4096]{1,0:T(8,128)(2,1)} async-done(((bf16[2048,4096]{1,0:T(8,128)(2,1)}), bf16[128,4096]{1,0:T(8,128)(2,1)}) %reduce-scatter.12.cloned.1.call-update) | async-done | bytes 1048592
  827.8 1.6 copy.12
  829.4 1.5 convert_element_type.31
  830.9 351.1 %reduce-scatter.10.cloned.1.call-done = bf16[128,4096]{1,0:T(8,128)(2,1)} async-done(((bf16[2048,4096]{1,0:T(8,128)(2,1)}), bf16[128,4096]{1,0:T(8,128)(2,1)}) %reduce-scatter.10.cloned.1.call-update) | async-done | bytes 1048592
  1182.0 1.6 copy.10
  1183.6 1.6 copy.8
  1185.3 14.9 %reduce-scatter.8.cloned.1.call-done = bf16[512,1024]{1,0:T(8,128)(2,1)} async-done(((bf16[512,2048]{1,0:T(8,128)(2,1)}), bf16[512,1024]{1,0:T(8,128)(2,1)}) %reduce-scatter.8.cloned.1.call-update) | async-done | bytes 1048592 | tf_op jit(solution)/shard_map/reduce_scatter | solution.py:35
  (10 shorter events, 0.2 us)
Async XLA Ops:
  7.2 15.7 %all-gather.5.cloned.1.call-start = ((), (), s32[]{:S(2)}) async-start(), calls=%async_computation.3 | async-start | bytes 3145728 | tf_op jit(solution)/shard_map/all_gather | solution.py:21
  7.9 209.9 %all-gather.7.cloned.1.call-start = ((), (), s32[]{:S(2)}) async-start(), calls=%async_computation.4 | async-start | bytes 17825792 | tf_op jit(solution)/shard_map/all_gather | solution.py:29
  8.6 224.1 %all-gather.9.cloned.1.call-start = ((), (), s32[]{:S(2)}) async-start(), calls=%async_computation.5 | async-start | bytes 3145728 | tf_op jit(solution)/shard_map/all_gather | solution.py:22
  9.4 471.7 %all-gather.11.cloned.1.call-start = ((), (), s32[]{:S(2)}) async-start(), calls=%async_computation.6 | async-start | bytes 17825792 | tf_op jit(solution)/shard_map/all_gather | solution.py:28
  10.0 817.9 %reduce-scatter.12.cloned.1.call-start = ((), (), s32[]{:S(2)}) async-start(), calls=%async_computation.9 | async-start | bytes 17825792
  270.5 226.2 %copy-start = (bf16[512,2048]{1,0:T(8,128)(2,1)S(1)}, bf16[512,2048]{1,0:T(8,128)(2,1)}, u32[]{:S(2)}) copy-start(bf16[512,2048]{1,0:T(8,128)(2,1)} %all-gather.5.cloned.1.call-done) | copy-start | bytes 6291460
  270.5 911.5 %reduce-scatter.10.cloned.1.call-start = ((), (), s32[]{:S(2)}) async-start(), calls=%async_computation.8 | async-start | bytes 17825792
  532.8 667.3 %reduce-scatter.8.cloned.1.call-start = ((), (), s32[]{:S(2)}) async-start(), calls=%async_computation.7 | async-start | bytes 3145728 | tf_op jit(solution)/shard_map/reduce_scatter | solution.py:35
Sparse Core Ops, SparseCore 0:
  9.5 13.2 all-gather.4
  25.6 192.1 all-gather.6
  219.4 8.7 all-gather.8
  230.7 250.2 all-gather.10
  483.2 344.5 reduce-scatter.11
  830.0 352.0 reduce-scatter.9
  1184.8 15.2 reduce-scatter.7
where the time goes:
time: 1210 us
  waiting for transfers between devices  1070 us (88%)
  matrix products  76.2 us (6%)
  local copies, waits for them, and re-layouts  47.8 us (4%)
  between operations  14.2 us (1%)
    unnamed x9, waiting for transfers between devices  634 us
    all_gather x1, waiting for transfers between devices, per_device(): lax.all_gather(down_weight, 'fs', axis=1, tiled=True)  210 us
    all_gather x1, waiting for transfers between devices, per_device(): whole_up = lax.all_gather(up_weight, 'fs', axis=0, tiled=True)  195 us
    unnamed x7, local copies, waits for them, and re-layouts  47.8 us
    dot_general x2, matrix products, left_product(): lax.dot_general(left, right, (((0,), (0,)), ((), ())), preferred_element_...  30.9 us
    dot_general x2, matrix products, right_product(): lax.dot_general(left, right, (((1,), (1,)), ((), ())), preferred_element_...  30.4 us
  transfers between devices with their start and end apart: 7, of which 6 were waited for; matrix products, arithmetic and copies ran while one was open for 10% of the time, Pallas kernels for 0%

commit v1 on v0

--- a/solution.py
+++ b/solution.py
@@ -25,7 +25,8 @@
     tokens = rows * lax.axis_size("fs")
     scale = lax.rsqrt(jnp.asarray(tokens, jnp.float32))
     block = whole_cot
-    act_grad = right_product(block, lax.all_gather(down_weight, "fs", axis=1, tiled=True))
+    open_the_core = lambda inputs: jnp.concatenate(lax.all_gather(inputs, "fs"), axis=1)
+    act_grad = right_product(block, open_the_core(down_weight))
     whole_up = lax.all_gather(up_weight, "fs", axis=0, tiled=True)
     pre = jnp.dot(whole_input, whole_up, preferred_element_type=jnp.float32)
     rectified = jax.nn.relu(pre)

time: 1210 us -> 1150 us (0.950)
  waiting for transfers between devices: 1070 us -> 991 us
  local copies, waits for them, and re-layouts: 47.8 us -> 69.5 us
    all_gather x1, waiting for transfers between devices: 210 us -> 153 us  [per_device(): lax.all_gather(inputs, 'fs')]
    reshape x0 -> x1, local copies, waits for them, and re-layouts: none -> 21.3 us  [per_device(): jnp.concatenate(lax.all_gather(inputs, 'fs'), axis=1)]
    unnamed x9, waiting for transfers between devices: 634 us -> 615 us
    unnamed x7 -> x11, local copies, waits for them, and re-layouts: 47.8 us -> 48.3 us
  transfers between devices with their start and end apart: 7 -> 7, of which waited for: 6 -> 6; matrix products, arithmetic and copies ran while one was open for 10% -> 12% of each run, Pallas kernels for 0% -> 0%
where the time goes in v1:
time: 1150 us
  waiting for transfers between devices  991 us (86%)
  matrix products  72.2 us (6%)
  local copies, waits for them, and re-layouts  69.5 us (6%)
  between operations  14.2 us (1%)
    unnamed x9, waiting for transfers between devices  615 us
    all_gather x1, waiting for transfers between devices, per_device(): whole_up = lax.all_gather(up_weight, 'fs', axis=0, tiled=True)  195 us
    all_gather x1, waiting for transfers between devices, per_device(): lax.all_gather(inputs, 'fs')  153 us
    unnamed x11, local copies, waits for them, and re-layouts  48.3 us
    dot_general x2, matrix products, left_product(): lax.dot_general(left, right, (((0,), (0,)), ((), ())), preferred_element_...  28.6 us
    dot_general x2, matrix products, right_product(): lax.dot_general(left, right, (((1,), (1,)), ((), ())), preferred_element_...  28.5 us
  transfers between devices with their start and end apart: 7, of which 6 were waited for; matrix products, arithmetic and copies ran while one was open for 12% of the time, Pallas kernels for 0%

profile of v1, /device:TPU:0, one launch (start us, length us, event | category | flops | bytes accessed | tf_op | source)
XLA Modules:
  0.0 1148.9 jit_solution(9772851425815069178)
XLA Ops:
  7.2 0.7 all-gather.6.cloned.1.call-update
  7.9 0.7 all-gather.8.cloned.1.call-update
  8.7 0.7 all-gather.10.cloned.1.call-update
  9.4 0.5 all-gather.12.cloned.1.call-update
  10.0 12.8 %all-gather.6.cloned.1.call-done = bf16[512,2048]{1,0:T(8,128)(2,1)} async-done(((bf16[512,1024]{1,0:T(8,128)(2,1)}), bf16[512,2048]{1,0:T(8,128)(2,1)}) %all-gather.6.cloned.1.call-update) | async-done | bytes 2097168 | tf_op jit(solution)/shard_map/all_gather | solution.py:21
  22.8 195.0 %all-gather.8.cloned.1.call-done = bf16[2048,4096]{1,0:T(8,128)(2,1)} async-done(((bf16[128,4096]{1,0:T(8,128)(2,1)}), bf16[2048,4096]{1,0:T(8,128)(2,1)}) %all-gather.8.cloned.1.call-update) | async-done | bytes 16777232 | tf_op jit(solution)/shard_map/all_gather | solution.py:30
  217.8 15.0 %fusion.3 = f32[512,4096]{1,0:T(8,128)} fusion(bf16[512,2048]{1,0:T(8,128)(2,1)} %all-gather.6.cloned.1.call-done, bf16[2048,4096]{1,0:T(8,128)(2,1)} %all-gather.8.cloned.1.call-done), kind=kOutput, calls=%fused_computation.8 | convolution fusion | flops 8589934592 | bytes 27262976 | tf_op jit(solution)/shard_map/dot_general | solution.py:31
  232.8 16.2 %multiply_convert_fusion = bf16[4096,2048]{1,0:T(8,128)(2,1)} fusion(bf16[512,2048]{1,0:T(8,128)(2,1)} %all-gather.10.cloned.1.call-done, f32[512,4096]{1,0:T(8,128)} %fusion.3), kind=kOutput, calls=%fused_computation | convolution fusion | flops 8613003264 | bytes 27262976 | tf_op jit(solution)/shard_map/dot_general | solution.py:14
  249.0 20.7 %copy.15 = bf16[4096,2048]{0,1:T(8,128)(2,1)} copy(bf16[4096,2048]{1,0:T(8,128)(2,1)} %multiply_convert_fusion) | data formatting | bytes 33554432
  269.9 153.1 %all-gather.12.cloned.1.call-done = bf16[65536,128]{1,0:T(8,128)(2,1)} async-done(((bf16[4096,128]{1,0:T(8,128)(2,1)}), bf16[65536,128]{1,0:T(8,128)(2,1)}) %all-gather.12.cloned.1.call-update) | async-done | bytes 16777232 | tf_op jit(solution)/shard_map/all_gather | solution.py:28
  423.0 21.3 %copy.11 = bf16[4096,16,128]{0,2,1:T(8,128)(2,1)} copy(bf16[4096,16,128]{2,0,1:T(8,128)(2,1)} %bitcast.19) | data formatting | bytes 33554432 | tf_op jit(solution)/shard_map/reshape | solution.py:28
  444.3 13.8 %multiply_convert_fusion.3 = bf16[512,4096]{1,0:T(8,128)(2,1)S(1)} fusion(f32[512,4096]{1,0:T(8,128)} %fusion.3, bf16[512,2048]{1,0:T(8,128)(2,1)S(1)} %copy-done.1, bf16[4096,2048]{0,1:T(8,128)(2,1)} %bitcast.20), kind=kOutput, calls=%fused_computation.4 | convolution fusion | flops 8598323200 | bytes 31457280 | tf_op jit(solution)/shard_map/dot_general | solution.py:8
  458.1 2.0 copy-done.2
  460.1 12.4 %fusion = bf16[2048,4096]{0,1:T(8,128)(2,1)} fusion(bf16[512,4096]{1,0:T(8,128)(2,1)S(1)} %multiply_convert_fusion.3, bf16[512,2048]{1,0:T(8,128)(2,1)S(1)} %copy-done), kind=kOutput, calls=%fused_computation.2 | convolution fusion | flops 8606711808 | bytes 23068672 | tf_op jit(solution)/shard_map/dot_general | solution.py:14
  472.5 20.8 %copy.13 = bf16[2048,4096]{1,0:T(8,128)(2,1)} copy(bf16[2048,4096]{0,1:T(8,128)(2,1)} %fusion) | data formatting | bytes 33554432
  493.3 0.3 reduce-scatter.8.cloned.1.call-start
  493.6 14.8 %convolution_convert_fusion = bf16[512,2048]{1,0:T(8,128)(2,1)} fusion(bf16[512,4096]{1,0:T(8,128)(2,1)} %copy-done.2, bf16[2048,4096]{1,0:T(8,128)(2,1)} %all-gather.8.cloned.1.call-done), kind=kOutput, calls=%fused_computation.6 | convolution fusion | flops 8590983168 | bytes 23068672 | tf_op jit(solution)/shard_map/dot_general | solution.py:8
  508.4 261.4 %reduce-scatter.12.cloned.1.call-done = bf16[128,4096]{1,0:T(8,128)(2,1)} async-done(((bf16[2048,4096]{1,0:T(8,128)(2,1)}), bf16[128,4096]{1,0:T(8,128)(2,1)}) %reduce-scatter.12.cloned.1.call-update) | async-done | bytes 1048592
  769.8 1.6 copy.16
  771.4 1.5 convert_element_type.31
  772.8 351.2 %reduce-scatter.10.cloned.1.call-done = bf16[128,4096]{1,0:T(8,128)(2,1)} async-done(((bf16[2048,4096]{1,0:T(8,128)(2,1)}), bf16[128,4096]{1,0:T(8,128)(2,1)}) %reduce-scatter.10.cloned.1.call-update) | async-done | bytes 1048592
  1124.0 1.6 copy.14
  1125.6 1.6 copy.12
  1127.2 14.9 %reduce-scatter.8.cloned.1.call-done = bf16[512,1024]{1,0:T(8,128)(2,1)} async-done(((bf16[512,2048]{1,0:T(8,128)(2,1)}), bf16[512,1024]{1,0:T(8,128)(2,1)}) %reduce-scatter.8.cloned.1.call-update) | async-done | bytes 1048592 | tf_op jit(solution)/shard_map/reduce_scatter | solution.py:36
  (15 shorter events, 0.5 us)
Async XLA Ops:
  7.2 15.7 %all-gather.6.cloned.1.call-start = ((), (), s32[]{:S(2)}) async-start(), calls=%async_computation.3 | async-start | bytes 3145728 | tf_op jit(solution)/shard_map/all_gather | solution.py:21
  7.9 209.9 %all-gather.8.cloned.1.call-start = ((), (), s32[]{:S(2)}) async-start(), calls=%async_computation.4 | async-start | bytes 17825792 | tf_op jit(solution)/shard_map/all_gather | solution.py:30
  8.6 224.1 %all-gather.10.cloned.1.call-start = ((), (), s32[]{:S(2)}) async-start(), calls=%async_computation.5 | async-start | bytes 3145728 | tf_op jit(solution)/shard_map/all_gather | solution.py:22
  9.4 413.6 %all-gather.12.cloned.1.call-start = ((), (), s32[]{:S(2)}) async-start(), calls=%async_computation.7 | async-start | bytes 17825792 | tf_op jit(solution)/shard_map/all_gather | solution.py:28
  10.0 759.8 %reduce-scatter.12.cloned.1.call-start = ((), (), s32[]{:S(2)}) async-start(), calls=%async_computation.9 | async-start | bytes 17825792
  269.7 854.3 %reduce-scatter.10.cloned.1.call-start = ((), (), s32[]{:S(2)}) async-start(), calls=%async_computation.8 | async-start | bytes 17825792
  423.0 21.3 %copy-start.1 = (bf16[512,2048]{1,0:T(8,128)(2,1)S(1)}, bf16[512,2048]{1,0:T(8,128)(2,1)}, u32[]{:S(2)}) copy-start(bf16[512,2048]{1,0:T(8,128)(2,1)} %all-gather.10.cloned.1.call-done) | copy-start | bytes 6291460
  444.3 15.8 %copy-start = (bf16[512,2048]{1,0:T(8,128)(2,1)S(1)}, bf16[512,2048]{1,0:T(8,128)(2,1)}, u32[]{:S(2)}) copy-start(bf16[512,2048]{1,0:T(8,128)(2,1)} %all-gather.6.cloned.1.call-done) | copy-start | bytes 6291460
  458.0 2.0 copy-start.2
  493.3 648.8 %reduce-scatter.8.cloned.1.call-start = ((), (), s32[]{:S(2)}) async-start(), calls=%async_computation.6 | async-start | bytes 3145728 | tf_op jit(solution)/shard_map/reduce_scatter | solution.py:36
Sparse Core Ops, SparseCore 0:
  9.5 13.2 all-gather.5
  25.6 192.1 all-gather.7
  219.4 8.7 all-gather.9
  230.8 192.1 all-gather.11
  425.1 344.5 reduce-scatter.11
  771.9 352.0 reduce-scatter.9
  1126.8 15.2 reduce-scatter.7
